TPU v7x, 32 devices: a whole 2x2x4 slice. The times are simulated.
32 devices in a mesh: ep: 8 (over z, y), tp: 4 (over x, core).
Axes of the slice: x: 2, y: 2, z: 4, core: 2. Of those that a mesh axis runs over, the one named last changes fastest.
Arguments:
- tokens: bfloat16 [128, 4096], P('ep'), may hold values from -6 to 6
- norm_gain: float32 [4096], replicated, may hold values from 0.1 to 1.9
- token_expert_index: int32 [128, 4], P('ep'), may hold values from 0 to 7, as said below
- group_prob: float32 [128], P('ep'), may hold values from 0.25 to 1
- expert_weight: float32 [128, 4], P('ep'), may hold values from 0.05 to 1
- w_gate: bfloat16 [8, 4096, 2048], P('ep', None, 'tp'), may hold values from -0.09375 to 0.09375
- w_up: bfloat16 [8, 4096, 2048], P('ep', None, 'tp'), may hold values from -0.09375 to 0.09375
- w_down: bfloat16 [8, 2048, 4096], P('ep', 'tp'), may hold values from -0.125 to 0.125
Outputs:
- mixed: bfloat16 [128, 4096], P('ep', 'tp')
Inputs may be any that keep to these rules, and one draw needn't show every extreme that they name: `token_expert_index`: each row names 4 different experts, all of one group: the group g holds experts g * 4 to (g + 1) * 4 - 1. The 16 rows of one index of ep name any one expert at most 16 times.
All inputs are finite; a program needn't handle non-finite values.
Results may differ from a plain program's by a relative error of at most 0.019.
Values may be sent and summed in bfloat16 or wider, within the bound.
A program may use at most 64 MiB of HBM per device.

v0:
```python
import jax
import jax.numpy as jnp
from jax import lax
from jax.sharding import PartitionSpec as P

GROUPS = 2


def body(tokens, norm_gain, token_expert_index, group_prob, expert_weight, w_gate, w_up, w_down):
    rows_here, width = tokens.shape
    topk = token_expert_index.shape[1]
    experts = lax.axis_size("ep")
    tp_count = lax.axis_size("tp")
    per_group = experts // GROUPS
    capacity = min(rows_here, max(2, rows_here * topk // max(per_group - topk, 1) + 1))
    xf = tokens.astype(jnp.float32)
    normed = (xf * lax.rsqrt(jnp.mean(xf * xf, axis=-1, keepdims=True) + 1e-06) * norm_gain).astype(
        jnp.bfloat16
    )
    gates = group_prob[:, None] * expert_weight / jnp.sum(expert_weight, axis=-1, keepdims=True)
    flattened_index = token_expert_index.reshape(-1)
    onehot = (flattened_index[:, None] == jnp.arange(experts, dtype=jnp.int32)[None, :]).astype(
        jnp.int32
    )
    earlier = jnp.cumsum(onehot, axis=0) - onehot
    slot_rank = jnp.sum(earlier * onehot, axis=1)
    place = flattened_index * capacity + slot_rank
    slots_total = experts * capacity
    select = (jnp.arange(slots_total, dtype=jnp.int32)[:, None] == place[None, :]).astype(
        jnp.float32
    )
    select = jnp.sum(select.reshape(slots_total, rows_here, topk), axis=2).astype(jnp.bfloat16)
    outgoing = jnp.dot(select, normed, preferred_element_type=jnp.float32).astype(jnp.bfloat16)
    share = width // tp_count
    arrived = lax.all_to_all(outgoing, "ep", split_axis=0, concat_axis=0, tiled=True)
    gate = jnp.dot(arrived, w_gate[0], preferred_element_type=jnp.float32)
    upper = jnp.dot(arrived, w_up[0], preferred_element_type=jnp.float32)
    hidden = (jax.nn.silu(gate) * upper).astype(jnp.bfloat16)
    partial_out = jnp.dot(hidden, w_down[0], preferred_element_type=jnp.float32)
    mine = lax.psum_scatter(partial_out.astype(jnp.bfloat16), "tp", scatter_dimension=1, tiled=True)
    returned = lax.all_to_all(mine, "ep", split_axis=0, concat_axis=0, tiled=True)
    picked = returned[place].astype(jnp.float32).reshape(rows_here, topk, share)
    mixed = jnp.sum(picked * gates[:, :, None], axis=1)
    return mixed.astype(jnp.bfloat16)


def solution(mesh):
    return jax.shard_map(
        body,
        mesh=mesh,
        in_specs=(
            P("ep", None),
            P(),
            P("ep", None),
            P("ep"),
            P("ep", None),
            P("ep", None, "tp"),
            P("ep", None, "tp"),
            P("ep", "tp", None),
        ),
        out_specs=P("ep", "tp"),
        check_vma=False,
    )
```

profile of v0, /device:TPU:0, one launch (start us, length us, event | category | flops | bytes accessed | tf_op | source)
XLA Modules:
  0.0 98.9 jit_solution(16778571858331678075)
XLA Ops:
  6.5 0.0 reduce-scatter.2.cloned.1.call-start
  6.5 0.8 copy.15
  7.3 0.1 eq.30
  7.4 0.1 fusion.25
  7.5 0.1 reduce_window_sum.11
  7.6 0.2 select_reduce_fusion
  7.7 0.1 reduce_sum.50
  7.8 0.1 copy.17
  7.9 0.1 convert_reduce_fusion
  8.0 1.1 %fusion.13 = f32[16]{0:T(128)S(1)} fusion(bf16[16,4096]{1,0:T(8,128)(2,1)} %param.8), kind=kLoop, calls=%fused_computation.12 | loop fusion | flops 196592 | bytes 131136 | tf_op jit(solution)/shard_map/reduce_sum | solution.py:17
  9.1 1.4 %convolution_convert_fusion.1 = bf16[128,4096]{1,0:T(8,128)(2,1)S(1)} fusion(bf16[16,4096]{1,0:T(8,128)(2,1)} %param.8, f32[4096]{0:T(1024)} %param.9, f32[16]{0:T(128)S(1)} %add_rsqrt_fusion, bf16[128,16]{0,1:T(8,128)(2,1)S(1)} %convert_reduce_fusion), kind=kOutput, calls=%fused_computation.2 | convolution fusion | flops 17563648 | bytes 1200192 | tf_op jit(solution)/shard_map/dot_general | solution.py:33
  10.5 32.9 %all_to_all.24 = bf16[8,16,4096]{2,1,0:T(8,128)(2,1)S(1)} all-to-all(bf16[8,16,4096]{2,1,0:T(8,128)(2,1)S(1)} %bitcast.31), channel_id=1, replica_groups=mesh['ep'=8,'tp'=4] {'ep'}, dimensions={0} | all-to-all | bytes 2097152 | tf_op jit(solution)/shard_map/all_to_all | solution.py:35
  43.3 2.9 %fusion.3 = f32[128,512]{1,0:T(8,128)S(1)} fusion(bf16[128,4096]{1,0:T(8,128)(2,1)S(1)} %bitcast.28, bf16[1,4096,512]{2,1,0:T(8,128)(2,1)} %param.13), kind=kOutput, calls=%fused_computation.6 | convolution fusion | flops 536870912 | bytes 5505024 | tf_op jit(solution)/shard_map/dot_general | solution.py:36
  46.3 0.0 copy-start
  46.3 0.0 copy-start.1
  46.3 5.9 %convolution_convert_fusion = bf16[128,4096]{1,0:T(8,128)(2,1)} fusion(bf16[1,512,4096]{2,1,0:T(8,128)(2,1)} %param.15, bf16[128,4096]{1,0:T(8,128)(2,1)S(1)} %bitcast.29, bf16[1,4096,512]{2,1,0:T(8,128)(2,1)} %param.14, f32[128,512]{1,0:T(8,128)S(1)} %fusion.3), kind=kOutput, calls=%fused_computation.1 | convolution fusion | flops 1074659328 | bytes 10747904 | tf_op jit(solution)/shard_map/dot_general | solution.py:39
  52.1 0.0 reduce-scatter.2.cloned.1.call-update
  52.2 0.1 mul.75
  52.2 0.0 copy-done
  52.3 23.8 %reduce-scatter.2.cloned.1.call-done = bf16[128,1024]{1,0:T(8,128)(2,1)} async-done(((bf16[128,4096]{1,0:T(8,128)(2,1)}), bf16[128,1024]{1,0:T(8,128)(2,1)}) %reduce-scatter.2.cloned.1.call-update) | async-done | bytes 262160 | tf_op jit(solution)/shard_map/reduce_scatter | solution.py:40
  76.1 5.5 %all-to-all-start.1 = ((bf16[8,16,1024]{2,1,0:T(8,128)(2,1)}), bf16[8,16,1024]{2,1,0:T(8,128)(2,1)S(1)}, u32[]{:S(2)}, u32[]{:S(2)}) async-start(bf16[8,16,1024]{2,1,0:T(8,128)(2,1)} %bitcast.32), calls=%async_computation.2 | async-start | bytes 524288 | tf_op jit(solution)/shard_map/all_to_all | solution.py:41
  81.6 0.0 copy-done.1
  81.7 0.1 copy.18
  81.8 8.6 %all-to-all-done.1 = bf16[8,16,1024]{2,1,0:T(8,128)(2,1)S(1)} async-done(((bf16[8,16,1024]{2,1,0:T(8,128)(2,1)}), bf16[8,16,1024]{2,1,0:T(8,128)(2,1)S(1)}, u32[]{:S(2)}, u32[]{:S(2)}) %all-to-all-start.1) | async-done | bytes 262176 | tf_op jit(solution)/shard_map/all_to_all | solution.py:41
  90.4 0.7 gather_fusion
  91.1 0.1 reshape.67
  91.2 0.9 multiply_reduce_fusion
  (6 shorter events, 0.1 us)
Async XLA Ops:
  6.5 69.6 %reduce-scatter.2.cloned.1.call-start = ((), (), s32[]{:S(2)}) async-start(), calls=%async_computation.3 | async-start | bytes 1310720 | tf_op jit(solution)/shard_map/reduce_scatter | solution.py:40
  46.3 6.0 %copy-start = (f32[16,4]{0,1:T(4,128)S(1)}, f32[16,4]{0,1:T(4,128)}, u32[]{:S(2)}) copy-start(f32[16,4]{0,1:T(4,128)} %param.12) | copy-start | bytes 772
  46.3 35.4 %copy-start.1 = (f32[16]{0:T(128)S(1)}, f32[16]{0:T(128)}, u32[]{:S(2)}) copy-start(f32[16]{0:T(128)} %param.11) | copy-start | bytes 196
  76.1 14.3 %all-to-all-start.1 = ((bf16[8,16,1024]{2,1,0:T(8,128)(2,1)}), bf16[8,16,1024]{2,1,0:T(8,128)(2,1)S(1)}, u32[]{:S(2)}, u32[]{:S(2)}) async-start(bf16[8,16,1024]{2,1,0:T(8,128)(2,1)} %bitcast.32), calls=%async_computation.2 | async-start | bytes 524288 | tf_op jit(solution)/shard_map/all_to_all | solution.py:41
Sparse Core Ops, SparseCore 0:
  52.3 23.7 reduce-scatter.1
where the time goes:
time: 99.2 us; the launch traced here: 98.9 us
  blocking collectives  32.9 us (33%)
  waiting for transfers between devices  32.5 us (33%)
  between operations  13.5 us (14%)
  matrix products  10.1 us (10%)
  starting transfers between devices  5.53 us (6%)
  other arithmetic  2.41 us (2%)
  local copies, waits for them, and re-layouts  1.98 us (2%)
    all_to_all x1, blocking collectives, body(): lax.all_to_all(outgoing, 'ep', split_axis=0, concat_axis=0, tiled=True)  32.9 us
    reduce_scatter x1, waiting for transfers between devices, body(): lax.psum_scatter(partial_out.astype(jnp.bfloat16), 'tp', scatter_dimensio...  23.8 us
    all_to_all x1, waiting for transfers between devices, body(): lax.all_to_all(mine, 'ep', split_axis=0, concat_axis=0, tiled=True)  8.63 us
    dot_general x1, matrix products, body(): partial_out = jnp.dot(hidden, w_down[0], preferred_element_type=jnp.float32)  5.86 us
    all_to_all x1, starting transfers between devices, body(): lax.all_to_all(mine, 'ep', split_axis=0, concat_axis=0, tiled=True)  5.52 us
    dot_general x1, matrix products, body(): gate = jnp.dot(arrived, w_gate[0], preferred_element_type=jnp.float32)  2.9 us
  transfers between devices with their start and end apart: 2, of which 2 were waited for; matrix products, arithmetic and copies ran while one was open for 0% of the time, Pallas kernels for 0%

commit v1 on v0

--- a/solution.py
+++ b/solution.py
@@ -1,12 +1,16 @@
+import functools
+
 import jax
 import jax.numpy as jnp
 from jax import lax
+from jax.experimental import pallas as pl
+from jax.experimental.pallas import tpu as pltpu
 from jax.sharding import PartitionSpec as P
 
 GROUPS = 2
 
 
-def body(tokens, norm_gain, token_expert_index, group_prob, expert_weight, w_gate, w_up, w_down):
+def general(tokens, norm_gain, token_expert_index, group_prob, expert_weight, w_gate, w_up, w_down):
     rows_here, width = tokens.shape
     topk = token_expert_index.shape[1]
     experts = lax.axis_size("ep")
@@ -44,6 +48,252 @@
     return mixed.astype(jnp.bfloat16)
 
 
+MESH = pl.DeviceIdType.MESH
+CHUNKS = 4
+LANES = 128
+
+
+def kernel(dims, tokens, gain, index, group_prob, weight, wg_hbm, wu_hbm, wd_hbm, out, xg, wg, wu, wd,
+           table, acc_g, acc_u, hid, csend, crecv, ckeep, xsend, xrecv, xkeep, ysend, yrecv, zsend, zrecv, zkeep,
+           wsem, gz, gy, gx, gc, gd, tz, ty, sc, sx, sy, sz):
+    nz, ny, rows, share, chunk = dims
+    ep, t = lax.axis_index("ep"), lax.axis_index("tp")
+    z, y = ep // ny, ep % ny
+    x, c = t // 2, t % 2
+    yo = 1 - y
+    t_core, t_x, t_diag = x * 2 + (1 - c), (1 - x) * 2 + c, (1 - x) * 2 + (1 - c)
+    half = nz * rows
+    y_dev = {"ep": z * ny + yo, "tp": t}
+    x_dev = {"ep": ep, "tp": t_x}
+    core_dev = {"ep": ep, "tp": t_core}
+
+    def z_dev(d):
+        return {"ep": ((z + d) % nz) * ny + y, "tp": t}
+
+    loads = [
+        pltpu.make_async_copy(wg_hbm.at[0], wg, wsem.at[0]),
+        pltpu.make_async_copy(wu_hbm.at[0], wu, wsem.at[1]),
+        pltpu.make_async_copy(wd_hbm.at[0], wd, wsem.at[2]),
+    ]
+    for load in loads:
+        load.start()
+
+    barrier = pltpu.get_barrier_semaphore()
+    peers = [z_dev(d) for d in range(1, nz)] + [y_dev, x_dev, core_dev]
+    for peer in peers:
+        pl.semaphore_signal(barrier, inc=1, device_id=peer, device_id_type=MESH)
+
+    def place(zz, yy):
+        return pl.ds(pl.multiple_of((yy * nz + zz) * rows, rows), rows)
+
+    xf = tokens[...].astype(jnp.float32)
+    scale = lax.rsqrt(jnp.mean(xf * xf, axis=-1, keepdims=True) + 1e-06)
+    normed = (xf * scale * gain[...]).astype(jnp.bfloat16)
+    for q in range(xg.shape[0]):
+        xg[q, place(z, y), :] = normed[:, q * share : (q + 1) * share]
+    ew = weight[...]
+    gates = group_prob[...] * ew / jnp.sum(ew, axis=-1, keepdims=True)
+    lane = lax.broadcasted_iota(jnp.int32, (rows, LANES), 1)
+    own = jnp.zeros((rows, LANES), jnp.float32)
+    for k in range(ew.shape[1]):
+        own = own + jnp.where(index[:, k : k + 1] == lane, gates[:, k : k + 1], 0.0)
+    table[place(z, y), :] = own
+    pl.semaphore_wait(barrier, len(peers))
+
+    sent = []
+
+    def send(src, dst, sems, i, device):
+        copy = pltpu.make_async_remote_copy(
+            src_ref=src, dst_ref=dst, send_sem=sems.at[0, i], recv_sem=sems.at[1, i],
+            device_id=device, device_id_type=MESH,
+        )
+        copy.start()
+        sent.append(copy)
+
+    def arrive(dst, sems, i):
+        pltpu.make_async_remote_copy(
+            src_ref=dst, dst_ref=dst, send_sem=sems.at[0, i], recv_sem=sems.at[1, i],
+            device_id=y_dev, device_id_type=MESH,
+        ).wait_recv()
+
+    def block(q, zz, yy):
+        return xg.at[q, place(zz, yy)]
+
+    def from_z(d):
+        return (z + nz - d) % nz
+
+    mine = block(t, z, y)
+    for d in range(1, nz):
+        send(mine, mine, gz, d, z_dev(d))
+    send(mine, mine, gy, 0, y_dev)
+    my_table = table.at[place(z, y)]
+    for d in range(1, nz):
+        send(my_table, my_table, tz, d, z_dev(d))
+    send(my_table, my_table, ty, 0, y_dev)
+
+    def spread(got, i):
+        send(got, got, gx, i, x_dev)
+        send(got, got, gc, i, core_dev)
+
+    got = block(t, z, yo)
+    arrive(got, gy, 0)
+    spread(got, nz)
+    for d in range(1, nz):
+        got = block(t, from_z(d), y)
+        arrive(got, gz, d)
+        send(got, got, gy, d, y_dev)
+        spread(got, d)
+    for d in range(1, nz):
+        got = block(t, from_z(d), yo)
+        arrive(got, gy, d)
+        spread(got, nz + d)
+    for d in range(1, nz):
+        got = table.at[place(from_z(d), y)]
+        arrive(got, tz, d)
+        send(got, got, ty, d, y_dev)
+
+    def which(i):
+        return (from_z(i % nz), y if i < nz else yo)
+
+    order = [nz] + list(range(1, nz)) + list(range(nz + 1, 2 * nz))
+
+    def project(q, first):
+        lhs = xg[q]
+        span = pl.ds(pl.multiple_of(q * share, share), share)
+        for acc, w in ((acc_g, wg), (acc_u, wu)):
+            value = jnp.dot(lhs, w[span, :], preferred_element_type=jnp.float32)
+            acc[...] = value if first else acc[...] + value
+
+    loads[0].wait()
+    loads[1].wait()
+    project(t, True)
+    for i in order:
+        got = block(t_x, *which(i))
+        arrive(got, gx, i)
+        send(got, got, gd, i, core_dev)
+    for i in order:
+        arrive(block(t_core, *which(i)), gc, i)
+    project(t_core, False)
+    project(t_x, False)
+    for d in range(nz):
+        arrive(table.at[place(from_z(d), yo)], ty, d)
+    for i in order:
+        arrive(block(t_diag, *which(i)), gd, i)
+    project(t_diag, False)
+
+    lanes = lax.broadcasted_iota(jnp.int32, table.shape, 1)
+    factor = jnp.sum(jnp.where(lanes == ep, table[...], 0.0), axis=1, keepdims=True)
+    gate = acc_g[...]
+    hid[...] = (gate / (1.0 + jnp.exp(-gate)) * acc_u[...] * factor).astype(jnp.bfloat16)
+
+    loads[2].wait()
+
+    def down(xq, cq, j):
+        start = pl.multiple_of((xq * 2 + cq) * share + j * chunk, chunk)
+        return jnp.dot(hid[...], wd[:, pl.ds(start, chunk)], preferred_element_type=jnp.float32)
+
+    for j in range(CHUNKS):
+        csend[0, j] = down(1 - x, 1 - c, j).astype(jnp.bfloat16)
+        send(csend.at[0, j], crecv.at[0, j], sc, j, core_dev)
+    for j in range(CHUNKS):
+        ckeep[0, j] = down(1 - x, c, j)
+    for j in range(CHUNKS):
+        arrive(crecv.at[0, j], sc, j)
+        xsend[j] = (ckeep[0, j] + crecv[0, j].astype(jnp.float32)).astype(jnp.bfloat16)
+        send(xsend.at[j], xrecv.at[j], sx, j, x_dev)
+    for j in range(CHUNKS):
+        csend[1, j] = down(x, 1 - c, j).astype(jnp.bfloat16)
+        send(csend.at[1, j], crecv.at[1, j], sc, CHUNKS + j, core_dev)
+    for j in range(CHUNKS):
+        ckeep[1, j] = down(x, c, j)
+    for j in range(CHUNKS):
+        arrive(crecv.at[1, j], sc, CHUNKS + j)
+        ckeep[1, j] = ckeep[1, j] + crecv[1, j].astype(jnp.float32)
+
+    ours, theirs = pl.ds(pl.multiple_of(y * half, half), half), pl.ds(pl.multiple_of(yo * half, half), half)
+
+    def after_x(j):
+        arrive(xrecv.at[j], sx, j)
+        ysend[j] = (ckeep[1, j, theirs, :] + xrecv[j, theirs, :].astype(jnp.float32)).astype(jnp.bfloat16)
+        send(ysend.at[j], yrecv.at[j], sy, j, y_dev)
+        xkeep[j] = ckeep[1, j, ours, :] + xrecv[j, ours, :].astype(jnp.float32)
+
+    def after_y(j):
+        arrive(yrecv.at[j], sy, j)
+        total = xkeep[j] + yrecv[j].astype(jnp.float32)
+        zkeep[j] = total
+        zsend[j] = total.astype(jnp.bfloat16)
+        for d in range(1, nz):
+            src = zsend.at[j, pl.ds(pl.multiple_of(((z + d) % nz) * rows, rows), rows)]
+            send(src, zrecv.at[j, d - 1], sz, j * nz + d, z_dev(d))
+
+    for j in range(CHUNKS):
+        after_x(j)
+        if j:
+            after_y(j - 1)
+    after_y(CHUNKS - 1)
+    for j in range(CHUNKS):
+        total = zkeep[j, pl.ds(pl.multiple_of(z * rows, rows), rows), :]
+        for d in range(1, nz):
+            arrive(zrecv.at[j, d - 1], sz, j * nz + d)
+            total = total + zrecv[j, d - 1].astype(jnp.float32)
+        out[:, j * chunk : (j + 1) * chunk] = total.astype(jnp.bfloat16)
+    for copy in sent:
+        copy.wait_send()
+
+
+def fused(tokens, norm_gain, token_expert_index, group_prob, expert_weight, w_gate, w_up, w_down):
+    rows, width = tokens.shape
+    n_ep, n_tp = lax.axis_size("ep"), lax.axis_size("tp")
+    ny = 2
+    nz = n_ep // ny
+    share, hidden = width // n_tp, w_gate.shape[2]
+    chunk = share // CHUNKS
+    all_rows = n_ep * rows
+    half = nz * rows
+    bf, f32 = jnp.bfloat16, jnp.float32
+    vmem, dma = pltpu.VMEM, pltpu.SemaphoreType.DMA
+    return pl.pallas_call(
+        functools.partial(kernel, (nz, ny, rows, share, chunk)),
+        out_shape=jax.ShapeDtypeStruct((rows, share), bf),
+        in_specs=[pl.BlockSpec(memory_space=vmem)] * 5 + [pl.BlockSpec(memory_space=pl.ANY)] * 3,
+        out_specs=pl.BlockSpec(memory_space=vmem),
+        scratch_shapes=[
+            vmem((n_tp, all_rows, share), bf),
+            vmem(w_gate.shape[1:], bf), vmem(w_up.shape[1:], bf), vmem(w_down.shape[1:], bf),
+            vmem((all_rows, LANES), f32),
+            vmem((all_rows, hidden), f32), vmem((all_rows, hidden), f32), vmem((all_rows, hidden), bf),
+            vmem((2, CHUNKS, all_rows, chunk), bf), vmem((2, CHUNKS, all_rows, chunk), bf),
+            vmem((2, CHUNKS, all_rows, chunk), f32),
+            vmem((CHUNKS, all_rows, chunk), bf), vmem((CHUNKS, all_rows, chunk), bf),
+            vmem((CHUNKS, half, chunk), f32),
+            vmem((CHUNKS, half, chunk), bf), vmem((CHUNKS, half, chunk), bf),
+            vmem((CHUNKS, half, chunk), bf), vmem((CHUNKS, nz - 1, rows, chunk), bf),
+            vmem((CHUNKS, half, chunk), f32),
+            dma((3,)), dma((2, nz)), dma((2, nz)), dma((2, 2 * nz)), dma((2, 2 * nz)), dma((2, 2 * nz)),
+            dma((2, nz)), dma((2, nz)),
+            dma((2, 2 * CHUNKS)), dma((2, CHUNKS)), dma((2, CHUNKS)), dma((2, CHUNKS * nz)),
+        ],
+        compiler_params=pltpu.CompilerParams(
+            collective_id=0, has_side_effects=True, vmem_limit_bytes=48 * 1024 * 1024
+        ),
+    )(tokens, norm_gain[None, :], token_expert_index, group_prob[:, None], expert_weight, w_gate, w_up, w_down)
+
+
+def slots(rows, topk, experts):
+    return min(rows, max(2, rows * topk // max(experts // GROUPS - topk, 1) + 1))
+
+
+def body(*args):
+    tokens, topk = args[0], args[2].shape[1]
+    n_ep, n_tp = lax.axis_size("ep"), lax.axis_size("tp")
+    rows, width = tokens.shape
+    dense = slots(rows, topk, n_ep) == rows and n_ep % 2 == 0 and n_ep <= LANES and n_tp == 4
+    if dense and rows % 16 == 0 and width % (n_tp * CHUNKS * LANES) == 0:
+        return fused(*args)
+    return general(*args)
+
+
 def solution(mesh):
     return jax.shard_map(
         body,

time: 99.2 us -> 43 us (0.43)
  Pallas kernels: 0 us -> 36.1 us
  blocking collectives: 32.9 us -> 0 us
  waiting for transfers between devices: 32.5 us -> 0 us
  between operations: 13.5 us -> 0.01 us
  matrix products: 10.1 us -> 0 us
  starting transfers between devices: 5.53 us -> 0 us
  local copies, waits for them, and re-layouts: 1.98 us -> 6.67 us
  other arithmetic: 2.41 us -> 0 us
    pallas_call x0 -> x1, Pallas kernels: none -> 36.1 us  [fused(): pl.pallas_call(functools.partial(kernel, (nz, ny, rows, share, chunk)), o...]
    all_to_all x1 -> x0, blocking collectives: 32.9 us -> none  [body(): lax.all_to_all(outgoing, 'ep', split_axis=0, concat_axis=0, tiled=True)]
    reduce_scatter x1 -> x0, waiting for transfers between devices: 23.8 us -> none  [body(): lax.psum_scatter(partial_out.astype(jnp.bfloat16), 'tp', scatter_dimensio...]
    dot_general x3 -> x0, matrix products: 10.1 us -> none  [the longest x1 5.86 us: body(): partial_out = jnp.dot(hidden, w_down[0], preferred_element_type=jnp.float32)]
    all_to_all x1 -> x0, waiting for transfers between devices: 8.63 us -> none  [body(): lax.all_to_all(mine, 'ep', split_axis=0, concat_axis=0, tiled=True)]
    all_to_all x1 -> x0, starting transfers between devices: 5.52 us -> none  [body(): lax.all_to_all(mine, 'ep', split_axis=0, concat_axis=0, tiled=True)]
    unnamed x5 -> x9, local copies, waits for them, and re-layouts: 0.77 us -> 5.94 us
    reduce_sum x5 -> x0, other arithmetic: 2.19 us -> none  [the longest x1 1.07 us: body(): jnp.mean(xf * xf, axis=-1, keepdims=True) + 1e-06]
  transfers between devices with their start and end apart: 2 -> 0, of which waited for: 2 -> 0; matrix products, arithmetic and copies ran while one was open for 0% -> 0% of each run, Pallas kernels for 0% -> 0%
where the time goes in v1:
time: 43 us; the launch traced here: 42.8 us
  Pallas kernels  36.1 us (84%)
  local copies, waits for them, and re-layouts  6.67 us (16%)
    pallas_call x1, Pallas kernels, fused(): pl.pallas_call(functools.partial(kernel, (nz, ny, rows, share, chunk)), o...  36.1 us
    unnamed x9, local copies, waits for them, and re-layouts  5.94 us

profile of v1, /device:TPU:0, one launch (start us, length us, event | category | flops | bytes accessed | tf_op | source)
XLA Modules:
  0.0 42.8 jit_solution(10321697854046012911)
XLA Ops:
  0.0 0.8 %copy.9.index = s32[16,4]{1,0:T(8,128)S(1)} copy(s32[16,4]{0,1:T(4,128)} %param.10) | data formatting | bytes 512 | tf_op args[2]
  0.8 0.7 %copy.10.group_prob = f32[16,1]{1,0:T(8,128)S(1)} copy(f32[16,1]{0,1:T(1,128)} %bitcast.3) | data formatting | bytes 128 | tf_op jit(solution)/shard_map/broadcast_in_dim | solution.py:280
  1.5 0.8 %copy.11.weight = f32[16,4]{1,0:T(8,128)S(1)} copy(f32[16,4]{0,1:T(4,128)} %param.12) | data formatting | bytes 512 | tf_op args[4]
  2.2 0.0 copy-start
  2.2 2.2 %copy-done = bf16[1,4096,512]{2,1,0:T(8,128)(2,1)S(1)} copy-done((bf16[1,4096,512]{2,1,0:T(8,128)(2,1)S(1)}, bf16[1,4096,512]{2,1,0:T(8,128)(2,1)}, u32[]{:S(2)}) %copy-start) | copy-done | bytes 4194328
  4.4 0.0 copy-start.1
  4.4 0.9 %copy-done.1 = bf16[16,4096]{1,0:T(8,128)(2,1)S(1)} copy-done((bf16[16,4096]{1,0:T(8,128)(2,1)S(1)}, bf16[16,4096]{1,0:T(8,128)(2,1)}, u32[]{:S(2)}) %copy-start.1) | copy-done | bytes 131096
  5.3 0.0 copy-start.2
  5.3 0.7 %copy-done.2 = f32[4096]{0:T(1024)S(1)} copy-done((f32[4096]{0:T(1024)S(1)}, f32[4096]{0:T(1024)}, u32[]{:S(2)}) %copy-start.2) | copy-done | bytes 16408
  6.1 36.1 %shard_map.82 = bf16[16,1024]{1,0:T(8,128)(2,1)S(1)} custom-call(bf16[16,4096]{1,0:T(8,128)(2,1)S(1)} %copy-done.1, f32[1,4096]{1,0:T(1,128)S(1)} %bitcast.2, s32[16,4]{1,0:T(8,128)S(1)} %copy.9.index, f32[16,1]{1,0:T(8,128)S(1)} %copy.10.group_prob, f32[16,4]{1,0:T(8,128)S(1)} %copy.11.weight, bf16[1,4096,512]{2,1,0:T(8,128)(2,1)S(1)} %copy-done, ...), custom_call_target="tpu_custom_call" | custom-call | tf_op jit(solution)/shard_map/pallas_call | solution.py:256
  42.1 0.6 %copy.13 = bf16[16,1024]{1,0:T(8,128)(2,1)} copy(bf16[16,1024]{1,0:T(8,128)(2,1)S(1)} %shard_map.82) | data formatting | bytes 65536
Async XLA Ops:
  2.2 2.2 %copy-start = (bf16[1,4096,512]{2,1,0:T(8,128)(2,1)S(1)}, bf16[1,4096,512]{2,1,0:T(8,128)(2,1)}, u32[]{:S(2)}) copy-start(bf16[1,4096,512]{2,1,0:T(8,128)(2,1)} %wg_hbm.1) | copy-start | bytes 12582916
  4.4 0.9 %copy-start.1 = (bf16[16,4096]{1,0:T(8,128)(2,1)S(1)}, bf16[16,4096]{1,0:T(8,128)(2,1)}, u32[]{:S(2)}) copy-start(bf16[16,4096]{1,0:T(8,128)(2,1)} %tokens.1) | copy-start | bytes 393220
  5.3 0.7 %copy-start.2 = (f32[4096]{0:T(1024)S(1)}, f32[4096]{0:T(1024)}, u32[]{:S(2)}) copy-start(f32[4096]{0:T(1024)} %param.9) | copy-start | bytes 49156

commit v2 on v1

--- a/solution.py
+++ b/solution.py
@@ -49,13 +49,13 @@
 
 
 MESH = pl.DeviceIdType.MESH
-CHUNKS = 4
+CHUNKS = 2
 LANES = 128
 
 
-def kernel(dims, tokens, gain, index, group_prob, weight, wg_hbm, wu_hbm, wd_hbm, out, xg, wg, wu, wd,
-           table, acc_g, acc_u, hid, csend, crecv, ckeep, xsend, xrecv, xkeep, ysend, yrecv, zsend, zrecv, zkeep,
-           wsem, gz, gy, gx, gc, gd, tz, ty, sc, sx, sy, sz):
+def kernel(dims, tokens_hbm, gain_hbm, index_hbm, prob_hbm, weight_hbm, wg_hbm, wu_hbm, wd_hbm, out,
+           tokens, gain, index, group_prob, weight, xg, wg, wu, wd, table, acc_g, acc_u, hid, csend, crecv, ckeep, bsend, ysend, brecv, zsend, zrecv, zkeep,
+           wsem, gz, gy, gx, gw, gc, gd, tz, ty, sc, sb, sz):
     nz, ny, rows, share, chunk = dims
     ep, t = lax.axis_index("ep"), lax.axis_index("tp")
     z, y = ep // ny, ep % ny
@@ -67,37 +67,53 @@
     x_dev = {"ep": ep, "tp": t_x}
     core_dev = {"ep": ep, "tp": t_core}
 
+    diag_dev = {"ep": z * ny + yo, "tp": t_x}
+
+    def flip(d):
+        return sum(
+            (1 << b) * (1 - (z // (1 << b)) % 2 if d >> b & 1 else (z // (1 << b)) % 2) for b in range(nz.bit_length() - 1)
+        )
+
     def z_dev(d):
-        return {"ep": ((z + d) % nz) * ny + y, "tp": t}
+        return {"ep": flip(d) * ny + y, "tp": t}
 
     loads = [
         pltpu.make_async_copy(wg_hbm.at[0], wg, wsem.at[0]),
         pltpu.make_async_copy(wu_hbm.at[0], wu, wsem.at[1]),
         pltpu.make_async_copy(wd_hbm.at[0], wd, wsem.at[2]),
     ]
-    for load in loads:
+    small = [
+        pltpu.make_async_copy(src, dst, wsem.at[3 + i])
+        for i, (src, dst) in enumerate(
+            ((tokens_hbm, tokens), (gain_hbm, gain), (index_hbm, index), (prob_hbm, group_prob), (weight_hbm, weight))
+        )
+    ]
+    for load in small + loads:
         load.start()
 
     barrier = pltpu.get_barrier_semaphore()
-    peers = [z_dev(d) for d in range(1, nz)] + [y_dev, x_dev, core_dev]
+    peers = [z_dev(d) for d in range(1, nz)] + [y_dev, x_dev, diag_dev, core_dev]
     for peer in peers:
         pl.semaphore_signal(barrier, inc=1, device_id=peer, device_id_type=MESH)
 
     def place(zz, yy):
         return pl.ds(pl.multiple_of((yy * nz + zz) * rows, rows), rows)
 
+    for load in small:
+        load.wait()
     xf = tokens[...].astype(jnp.float32)
     scale = lax.rsqrt(jnp.mean(xf * xf, axis=-1, keepdims=True) + 1e-06)
     normed = (xf * scale * gain[...]).astype(jnp.bfloat16)
     for q in range(xg.shape[0]):
         xg[q, place(z, y), :] = normed[:, q * share : (q + 1) * share]
     ew = weight[...]
-    gates = group_prob[...] * ew / jnp.sum(ew, axis=-1, keepdims=True)
-    lane = lax.broadcasted_iota(jnp.int32, (rows, LANES), 1)
-    own = jnp.zeros((rows, LANES), jnp.float32)
-    for k in range(ew.shape[1]):
-        own = own + jnp.where(index[:, k : k + 1] == lane, gates[:, k : k + 1], 0.0)
-    table[place(z, y), :] = own
+    gates = group_prob[...] * ew / jnp.sum(ew, axis=0, keepdims=True)
+    expert = lax.broadcasted_iota(jnp.int32, (table.shape[1], rows), 0)
+    own = jnp.zeros(expert.shape, jnp.float32)
+    for k in range(ew.shape[0]):
+        own = own + jnp.where(index[k : k + 1, :] == expert, gates[k : k + 1, :], 0.0)
+    table[y * nz + z] = jnp.zeros(table.shape[1:], jnp.float32)
+    table[y * nz + z, :, :rows] = own
     pl.semaphore_wait(barrier, len(peers))
 
     sent = []
@@ -119,41 +135,37 @@
     def block(q, zz, yy):
         return xg.at[q, place(zz, yy)]
 
-    def from_z(d):
-        return (z + nz - d) % nz
-
     mine = block(t, z, y)
-    for d in range(1, nz):
+    for d in range(nz - 1, 0, -1):
         send(mine, mine, gz, d, z_dev(d))
     send(mine, mine, gy, 0, y_dev)
-    my_table = table.at[place(z, y)]
+    other = block(t_x, z, y)
+    send(other, other, gy, nz, y_dev)
+    my_table = table.at[y * nz + z]
     for d in range(1, nz):
         send(my_table, my_table, tz, d, z_dev(d))
     send(my_table, my_table, ty, 0, y_dev)
 
-    def spread(got, i):
-        send(got, got, gx, i, x_dev)
-        send(got, got, gc, i, core_dev)
-
-    got = block(t, z, yo)
-    arrive(got, gy, 0)
-    spread(got, nz)
-    for d in range(1, nz):
-        got = block(t, from_z(d), y)
+    def relay(got, sems, i, onward, k):
+        arrive(got, sems, i)
+        send(got, got, onward, k, core_dev)
+
+    relay(block(t, z, yo), gy, 0, gc, nz)
+    relay(block(t_x, z, yo), gy, nz, gd, nz)
+    for d in range(1, nz):
+        got = block(t, flip(d), y)
         arrive(got, gz, d)
+        send(got, got, gw, d, diag_dev)
         send(got, got, gy, d, y_dev)
-        spread(got, d)
-    for d in range(1, nz):
-        got = block(t, from_z(d), yo)
-        arrive(got, gy, d)
-        spread(got, nz + d)
-    for d in range(1, nz):
-        got = table.at[place(from_z(d), y)]
+        send(got, got, gx, d, x_dev)
+        send(got, got, gc, d, core_dev)
+    for d in range(1, nz):
+        got = table.at[y * nz + flip(d)]
         arrive(got, tz, d)
         send(got, got, ty, d, y_dev)
 
     def which(i):
-        return (from_z(i % nz), y if i < nz else yo)
+        return (flip(i % nz), y if i < nz else yo)
 
     order = [nz] + list(range(1, nz)) + list(range(nz + 1, 2 * nz))
 
@@ -166,23 +178,30 @@
 
     loads[0].wait()
     loads[1].wait()
+    for d in range(1, nz):
+        relay(block(t_x, flip(d), y), gx, d, gd, d)
+        relay(block(t, flip(d), yo), gy, d, gc, nz + d)
     project(t, True)
-    for i in order:
-        got = block(t_x, *which(i))
-        arrive(got, gx, i)
-        send(got, got, gd, i, core_dev)
+    for d in range(1, nz):
+        relay(block(t_x, flip(d), yo), gw, d, gd, nz + d)
     for i in order:
         arrive(block(t_core, *which(i)), gc, i)
     project(t_core, False)
     project(t_x, False)
     for d in range(nz):
-        arrive(table.at[place(from_z(d), yo)], ty, d)
+        arrive(table.at[yo * nz + flip(d)], ty, d)
     for i in order:
         arrive(block(t_diag, *which(i)), gd, i)
     project(t_diag, False)
 
-    lanes = lax.broadcasted_iota(jnp.int32, table.shape, 1)
-    factor = jnp.sum(jnp.where(lanes == ep, table[...], 0.0), axis=1, keepdims=True)
+    diagonal = lax.broadcasted_iota(jnp.int32, (rows, rows), 0) == lax.broadcasted_iota(jnp.int32, (rows, rows), 1)
+    factor = jnp.concatenate(
+        [
+            jnp.sum(jnp.where(diagonal, table[b, pl.ds(ep, 1), :rows], 0.0), axis=1, keepdims=True)
+            for b in range(table.shape[0])
+        ],
+        axis=0,
+    )
     gate = acc_g[...]
     hid[...] = (gate / (1.0 + jnp.exp(-gate)) * acc_u[...] * factor).astype(jnp.bfloat16)
 
@@ -192,6 +211,7 @@
         start = pl.multiple_of((xq * 2 + cq) * share + j * chunk, chunk)
         return jnp.dot(hid[...], wd[:, pl.ds(start, chunk)], preferred_element_type=jnp.float32)
 
+    ours, theirs = pl.ds(pl.multiple_of(y * half, half), half), pl.ds(pl.multiple_of(yo * half, half), half)
     for j in range(CHUNKS):
         csend[0, j] = down(1 - x, 1 - c, j).astype(jnp.bfloat16)
         send(csend.at[0, j], crecv.at[0, j], sc, j, core_dev)
@@ -199,8 +219,9 @@
         ckeep[0, j] = down(1 - x, c, j)
     for j in range(CHUNKS):
         arrive(crecv.at[0, j], sc, j)
-        xsend[j] = (ckeep[0, j] + crecv[0, j].astype(jnp.float32)).astype(jnp.bfloat16)
-        send(xsend.at[j], xrecv.at[j], sx, j, x_dev)
+        bsend[j] = (ckeep[0, j] + crecv[0, j].astype(jnp.float32)).astype(jnp.bfloat16)
+        send(bsend.at[j, theirs], brecv.at[1, j], sb, CHUNKS + j, diag_dev)
+        send(bsend.at[j, ours], brecv.at[0, j], sb, j, x_dev)
     for j in range(CHUNKS):
         csend[1, j] = down(x, 1 - c, j).astype(jnp.bfloat16)
         send(csend.at[1, j], crecv.at[1, j], sc, CHUNKS + j, core_dev)
@@ -208,30 +229,19 @@
         ckeep[1, j] = down(x, c, j)
     for j in range(CHUNKS):
         arrive(crecv.at[1, j], sc, CHUNKS + j)
-        ckeep[1, j] = ckeep[1, j] + crecv[1, j].astype(jnp.float32)
-
-    ours, theirs = pl.ds(pl.multiple_of(y * half, half), half), pl.ds(pl.multiple_of(yo * half, half), half)
-
-    def after_x(j):
-        arrive(xrecv.at[j], sx, j)
-        ysend[j] = (ckeep[1, j, theirs, :] + xrecv[j, theirs, :].astype(jnp.float32)).astype(jnp.bfloat16)
-        send(ysend.at[j], yrecv.at[j], sy, j, y_dev)
-        xkeep[j] = ckeep[1, j, ours, :] + xrecv[j, ours, :].astype(jnp.float32)
-
-    def after_y(j):
-        arrive(yrecv.at[j], sy, j)
-        total = xkeep[j] + yrecv[j].astype(jnp.float32)
+        ysend[j] = (ckeep[1, j, theirs, :] + crecv[1, j, theirs, :].astype(jnp.float32)).astype(jnp.bfloat16)
+        send(ysend.at[j], brecv.at[2, j], sb, 2 * CHUNKS + j, y_dev)
+        zkeep[j] = ckeep[1, j, ours, :] + crecv[1, j, ours, :].astype(jnp.float32)
+    for j in range(CHUNKS):
+        total = zkeep[j]
+        for k in range(3):
+            arrive(brecv.at[k, j], sb, k * CHUNKS + j)
+            total = total + brecv[k, j].astype(jnp.float32)
         zkeep[j] = total
         zsend[j] = total.astype(jnp.bfloat16)
-        for d in range(1, nz):
-            src = zsend.at[j, pl.ds(pl.multiple_of(((z + d) % nz) * rows, rows), rows)]
+        for d in range(nz - 1, 0, -1):
+            src = zsend.at[j, pl.ds(pl.multiple_of(flip(d) * rows, rows), rows)]
             send(src, zrecv.at[j, d - 1], sz, j * nz + d, z_dev(d))
-
-    for j in range(CHUNKS):
-        after_x(j)
-        if j:
-            after_y(j - 1)
-    after_y(CHUNKS - 1)
     for j in range(CHUNKS):
         total = zkeep[j, pl.ds(pl.multiple_of(z * rows, rows), rows), :]
         for d in range(1, nz):
@@ -245,6 +255,7 @@
 def fused(tokens, norm_gain, token_expert_index, group_prob, expert_weight, w_gate, w_up, w_down):
     rows, width = tokens.shape
     n_ep, n_tp = lax.axis_size("ep"), lax.axis_size("tp")
+    topk = token_expert_index.shape[1]
     ny = 2
     nz = n_ep // ny
     share, hidden = width // n_tp, w_gate.shape[2]
@@ -256,28 +267,28 @@
     return pl.pallas_call(
         functools.partial(kernel, (nz, ny, rows, share, chunk)),
         out_shape=jax.ShapeDtypeStruct((rows, share), bf),
-        in_specs=[pl.BlockSpec(memory_space=vmem)] * 5 + [pl.BlockSpec(memory_space=pl.ANY)] * 3,
+        in_specs=[pl.BlockSpec(memory_space=pltpu.HBM)] * 8,
         out_specs=pl.BlockSpec(memory_space=vmem),
         scratch_shapes=[
+            vmem((rows, width), bf), vmem((1, width), f32), vmem((topk, rows), jnp.int32),
+            vmem((1, rows), f32), vmem((topk, rows), f32),
             vmem((n_tp, all_rows, share), bf),
             vmem(w_gate.shape[1:], bf), vmem(w_up.shape[1:], bf), vmem(w_down.shape[1:], bf),
-            vmem((all_rows, LANES), f32),
+            vmem((n_ep, n_ep, LANES), f32),
             vmem((all_rows, hidden), f32), vmem((all_rows, hidden), f32), vmem((all_rows, hidden), bf),
             vmem((2, CHUNKS, all_rows, chunk), bf), vmem((2, CHUNKS, all_rows, chunk), bf),
             vmem((2, CHUNKS, all_rows, chunk), f32),
-            vmem((CHUNKS, all_rows, chunk), bf), vmem((CHUNKS, all_rows, chunk), bf),
-            vmem((CHUNKS, half, chunk), f32),
-            vmem((CHUNKS, half, chunk), bf), vmem((CHUNKS, half, chunk), bf),
+            vmem((CHUNKS, all_rows, chunk), bf), vmem((CHUNKS, half, chunk), bf), vmem((3, CHUNKS, half, chunk), bf),
             vmem((CHUNKS, half, chunk), bf), vmem((CHUNKS, nz - 1, rows, chunk), bf),
             vmem((CHUNKS, half, chunk), f32),
-            dma((3,)), dma((2, nz)), dma((2, nz)), dma((2, 2 * nz)), dma((2, 2 * nz)), dma((2, 2 * nz)),
+            dma((8,)), dma((2, nz)), dma((2, nz + 1)), dma((2, nz)), dma((2, nz)), dma((2, 2 * nz)), dma((2, 2 * nz)),
             dma((2, nz)), dma((2, nz)),
-            dma((2, 2 * CHUNKS)), dma((2, CHUNKS)), dma((2, CHUNKS)), dma((2, CHUNKS * nz)),
+            dma((2, 2 * CHUNKS)), dma((2, 3 * CHUNKS)), dma((2, CHUNKS * nz)),
         ],
         compiler_params=pltpu.CompilerParams(
-            collective_id=0, has_side_effects=True, vmem_limit_bytes=48 * 1024 * 1024
+            collective_id=0, has_side_effects=True, vmem_limit_bytes=67043328
         ),
-    )(tokens, norm_gain[None, :], token_expert_index, group_prob[:, None], expert_weight, w_gate, w_up, w_down)
+    )(tokens, norm_gain[None, :], token_expert_index.T, group_prob[None, :], expert_weight.T, w_gate, w_up, w_down)
 
 
 def slots(rows, topk, experts):
@@ -288,7 +299,7 @@
     tokens, topk = args[0], args[2].shape[1]
     n_ep, n_tp = lax.axis_size("ep"), lax.axis_size("tp")
     rows, width = tokens.shape
-    dense = slots(rows, topk, n_ep) == rows and n_ep % 2 == 0 and n_ep <= LANES and n_tp == 4
+    dense = slots(rows, topk, n_ep) == rows and n_ep > 1 and n_ep & (n_ep - 1) == 0 and n_tp == 4
     if dense and rows % 16 == 0 and width % (n_tp * CHUNKS * LANES) == 0:
         return fused(*args)
     return general(*args)

time: 43 us -> 33 us (0.77)
  local copies, waits for them, and re-layouts: 6.67 us -> 1.38 us
  Pallas kernels: 36.1 us -> 31.5 us
    pallas_call x1, Pallas kernels: 36.1 us -> 31.5 us  [fused(): pl.pallas_call(functools.partial(kernel, (nz, ny, rows, share, chunk)), o...]
    unnamed x9 -> x1, local copies, waits for them, and re-layouts: 5.94 us -> 1.38 us
    broadcast_in_dim x1 -> x0, local copies, waits for them, and re-layouts: 0.73 us -> none  [fused(): group_prob[:, None]]
where the time goes in v2:
time: 33 us; the launch traced here: 32.9 us
  Pallas kernels  31.5 us (95%)
  local copies, waits for them, and re-layouts  1.38 us (4%)
    pallas_call x1, Pallas kernels, fused(): pl.pallas_call(functools.partial(kernel, (nz, ny, rows, share, chunk)), o...  31.5 us
    unnamed x1, local copies, waits for them, and re-layouts  1.38 us

profile of v2, /device:TPU:0, one launch (start us, length us, event | category | flops | bytes accessed | tf_op | source)
XLA Modules:
  0.0 32.9 jit_solution(1255780115845921920)
XLA Ops:
  0.0 31.5 %shard_map.82 = bf16[16,1024]{1,0:T(8,128)(2,1)} custom-call(bf16[16,4096]{1,0:T(8,128)(2,1)} %tokens_hbm.1, f32[1,4096]{1,0:T(1,128)} %bitcast.4, s32[4,16]{1,0:T(4,128)} %bitcast.5, f32[1,16]{1,0:T(1,128)} %bitcast.7, f32[4,16]{1,0:T(4,128)} %bitcast.6, bf16[1,4096,512]{2,1,0:T(8,128)(2,1)} %wg_hbm.1, bf16[1,4096,512]{2,1,0:T(8,128)(2,1)} %wu_hbm.1, ...), custom_call_target="tpu_custom_call" | custom-call | tf_op jit(solution)/shard_map/pallas_call | solution.py:267
  31.5 1.4 %copy.10 = bf16[16,1024]{1,0:T(8,128)(2,1)} copy(bf16[16,1024]{1,0:T(8,128)(2,1)} %shard_map.82) | data formatting | bytes 65536

commit v3 on v2

--- a/solution.py
+++ b/solution.py
@@ -77,6 +77,11 @@
     def z_dev(d):
         return {"ep": flip(d) * ny + y, "tp": t}
 
+    barrier = pltpu.get_barrier_semaphore()
+    peers = [z_dev(d) for d in range(1, nz)] + [y_dev, x_dev, diag_dev, core_dev]
+    for peer in peers:
+        pl.semaphore_signal(barrier, inc=1, device_id=peer, device_id_type=MESH)
+
     loads = [
         pltpu.make_async_copy(wg_hbm.at[0], wg, wsem.at[0]),
         pltpu.make_async_copy(wu_hbm.at[0], wu, wsem.at[1]),
@@ -90,11 +95,6 @@
     ]
     for load in small + loads:
         load.start()
-
-    barrier = pltpu.get_barrier_semaphore()
-    peers = [z_dev(d) for d in range(1, nz)] + [y_dev, x_dev, diag_dev, core_dev]
-    for peer in peers:
-        pl.semaphore_signal(barrier, inc=1, device_id=peer, device_id_type=MESH)
 
     def place(zz, yy):
         return pl.ds(pl.multiple_of((yy * nz + zz) * rows, rows), rows)
@@ -136,7 +136,7 @@
         return xg.at[q, place(zz, yy)]
 
     mine = block(t, z, y)
-    for d in range(nz - 1, 0, -1):
+    for d in range(1, nz):
         send(mine, mine, gz, d, z_dev(d))
     send(mine, mine, gy, 0, y_dev)
     other = block(t_x, z, y)
@@ -215,19 +215,15 @@
     for j in range(CHUNKS):
         csend[0, j] = down(1 - x, 1 - c, j).astype(jnp.bfloat16)
         send(csend.at[0, j], crecv.at[0, j], sc, j, core_dev)
+        csend[1, j] = down(x, 1 - c, j).astype(jnp.bfloat16)
+        send(csend.at[1, j], crecv.at[1, j], sc, CHUNKS + j, core_dev)
     for j in range(CHUNKS):
         ckeep[0, j] = down(1 - x, c, j)
-    for j in range(CHUNKS):
+        ckeep[1, j] = down(x, c, j)
         arrive(crecv.at[0, j], sc, j)
         bsend[j] = (ckeep[0, j] + crecv[0, j].astype(jnp.float32)).astype(jnp.bfloat16)
         send(bsend.at[j, theirs], brecv.at[1, j], sb, CHUNKS + j, diag_dev)
         send(bsend.at[j, ours], brecv.at[0, j], sb, j, x_dev)
-    for j in range(CHUNKS):
-        csend[1, j] = down(x, 1 - c, j).astype(jnp.bfloat16)
-        send(csend.at[1, j], crecv.at[1, j], sc, CHUNKS + j, core_dev)
-    for j in range(CHUNKS):
-        ckeep[1, j] = down(x, c, j)
-    for j in range(CHUNKS):
         arrive(crecv.at[1, j], sc, CHUNKS + j)
         ysend[j] = (ckeep[1, j, theirs, :] + crecv[1, j, theirs, :].astype(jnp.float32)).astype(jnp.bfloat16)
         send(ysend.at[j], brecv.at[2, j], sb, 2 * CHUNKS + j, y_dev)

time: 33 us -> 32.2 us (0.976)
  Pallas kernels: 31.5 us -> 30.6 us
    pallas_call x1, Pallas kernels: 31.5 us -> 30.6 us  [fused(): pl.pallas_call(functools.partial(kernel, (nz, ny, rows, share, chunk)), o...]
where the time goes in v3:
time: 32.2 us; the launch traced here: 32 us
  Pallas kernels  30.6 us (95%)
  local copies, waits for them, and re-layouts  1.38 us (4%)
    pallas_call x1, Pallas kernels, fused(): pl.pallas_call(functools.partial(kernel, (nz, ny, rows, share, chunk)), o...  30.6 us
    unnamed x1, local copies, waits for them, and re-layouts  1.38 us

profile of v3, /device:TPU:0, one launch (start us, length us, event | category | flops | bytes accessed | tf_op | source)
XLA Modules:
  0.0 32.0 jit_solution(752304982964230314)
XLA Ops:
  0.0 30.6 %shard_map.82 = bf16[16,1024]{1,0:T(8,128)(2,1)} custom-call(bf16[16,4096]{1,0:T(8,128)(2,1)} %tokens_hbm.1, f32[1,4096]{1,0:T(1,128)} %bitcast.4, s32[4,16]{1,0:T(4,128)} %bitcast.5, f32[1,16]{1,0:T(1,128)} %bitcast.7, f32[4,16]{1,0:T(4,128)} %bitcast.6, bf16[1,4096,512]{2,1,0:T(8,128)(2,1)} %wg_hbm.1, bf16[1,4096,512]{2,1,0:T(8,128)(2,1)} %wu_hbm.1, ...), custom_call_target="tpu_custom_call" | custom-call | tf_op jit(solution)/shard_map/pallas_call | solution.py:263
  30.6 1.4 %copy.10 = bf16[16,1024]{1,0:T(8,128)(2,1)} copy(bf16[16,1024]{1,0:T(8,128)(2,1)} %shard_map.82) | data formatting | bytes 65536
